TPU v7x, 32 devices: a whole 2x2x4 slice. The times are simulated.
32 devices in a mesh: grp: 2 (over x), ep: 16 (over z, y, core).
Axes of the slice: x: 2, y: 2, z: 4, core: 2. Of those that a mesh axis runs over, the one named last changes fastest.
Arguments:
- stream: bfloat16 [8192, 2048], P(('grp', 'ep')), parts along dimension 0, may hold values from -6 to 6
- norm_gain: float32 [2048], replicated, may hold values from 0.1 to 1.9
- routing: int32 [8192, 4], P(('grp', 'ep')), parts along dimension 0, may hold values from 0 to 31, all different within a row; in each aligned block of 256 rows (0 to 255, 256 to 511, ...) at most 64 rows name the same one
- gates: float32 [8192, 4], P(('grp', 'ep')), parts along dimension 0, may hold values from 0.1 to 1
- w_gate: bfloat16 [32, 2048, 512], P('ep'), may hold values from -0.125 to 0.125
- w_up: bfloat16 [32, 2048, 512], P('ep'), may hold values from -0.125 to 0.125
- w_down: bfloat16 [32, 512, 2048], P('ep'), may hold values from -0.25 to 0.25
- shared_gate: bfloat16 [2048, 512], replicated, may hold values from -0.125 to 0.125
- shared_up: bfloat16 [2048, 512], replicated, may hold values from -0.125 to 0.125
- shared_down: bfloat16 [512, 2048], replicated, may hold values from -0.25 to 0.25
Outputs:
- mixed: bfloat16 [8192, 2048], P(('grp', 'ep')), parts along dimension 0
There are 2 independent parts, one for each index of `grp`. A program takes and returns all parts, laid end to end along the dimension named above; an argument that names none is the same for every part. Nothing has to cross between parts.
Inputs may be any that keep to these rules, and one draw needn't show every extreme that they name: `routing`: each token names 4 different experts. Among the 256 tokens of one index of ep no expert is named more than 64 times, and on some index an expert is named exactly 64 times.
All inputs are finite; a program needn't handle non-finite values.
Results may differ from a plain program's by a relative error of at most 0.007.
Values may be sent and summed in bfloat16 or wider, within the bound.
A program may use at most 128 MiB of HBM per device.

v0:
```python
import functools
import jax
import jax.numpy as jnp
from jax import lax
from jax.experimental import pallas as pl
from jax.experimental.pallas import tpu as pltpu
from jax.sharding import PartitionSpec as P


def layer_norm(stream, norm_gain):
    widened = stream.astype(jnp.float32)
    row_mean = jnp.mean(widened, axis=-1, keepdims=True)
    variance = jnp.mean(jnp.square(widened - row_mean), axis=-1, keepdims=True)
    return ((widened - row_mean) * lax.rsqrt(variance + 1e-05) * norm_gain).astype(jnp.bfloat16)


def shared_branch(normed, shared_gate, shared_up, shared_down):
    shared_hidden = (
        jax.nn.silu(jnp.dot(normed, shared_gate, preferred_element_type=jnp.float32))
        * jnp.dot(normed, shared_up, preferred_element_type=jnp.float32)
    ).astype(jnp.bfloat16)
    return jnp.dot(shared_hidden, shared_down, preferred_element_type=jnp.float32)


def serve_rows(received, w_gate, w_up, w_down):
    local_count = w_gate.shape[0]
    blocks = received.reshape((-1, local_count) + received.shape[1:])
    gate_act = jnp.einsum("sxcd,xdh->sxch", blocks, w_gate, preferred_element_type=jnp.float32)
    up_act = jnp.einsum("sxcd,xdh->sxch", blocks, w_up, preferred_element_type=jnp.float32)
    hidden = (jax.nn.silu(gate_act) * up_act).astype(jnp.bfloat16)
    produced = jnp.einsum(
        "sxch,xhd->sxcd", hidden, w_down, preferred_element_type=jnp.float32
    ).astype(jnp.bfloat16)
    return lax.all_to_all(
        produced.reshape(received.shape), "ep", split_axis=0, concat_axis=0, tiled=True
    )


def generic_device(
    stream, norm_gain, routing, gates, w_gate, w_up, w_down, shared_gate, shared_up, shared_down
):
    tok_rows, top_count = routing.shape
    local_count = w_gate.shape[0]
    peer_count = lax.axis_size("ep")
    experts = local_count * peer_count
    capacity = 2 * tok_rows * top_count // experts
    normed = layer_norm(stream, norm_gain)
    row_ids = jnp.arange(tok_rows, dtype=jnp.int32)
    lower = (row_ids[:, None] > row_ids[None, :]).astype(jnp.bfloat16)
    slot_ids = jnp.arange(capacity, dtype=jnp.int32).astype(jnp.float32)
    expert_hits = (
        routing[:, :, None] == jnp.arange(experts, dtype=jnp.int32)[None, None, :]
    ).astype(jnp.float32)
    token_hits = jnp.sum(expert_hits, axis=1).astype(jnp.bfloat16)
    earlier = jnp.dot(lower, token_hits, preferred_element_type=jnp.float32)
    slot_index = jnp.sum(earlier[:, None, :] * expert_hits, axis=2)
    slot_hits = (slot_index[:, :, None] == slot_ids[None, None, :]).astype(jnp.float32)
    gate_table = jnp.sum(
        gates[:, :, None, None] * expert_hits[:, :, :, None] * slot_hits[:, :, None, :], axis=1
    )
    all_normed = lax.all_gather(normed, "ep", axis=0, tiled=True)
    all_routing = lax.all_gather(routing, "ep", axis=0, tiled=True)
    first_expert = lax.axis_index("ep") * local_count
    shifted = all_routing.reshape(peer_count, tok_rows, top_count) - first_expert
    local_hits = (
        shifted[:, :, :, None] == jnp.arange(local_count, dtype=jnp.int32)[None, None, None, :]
    ).astype(jnp.float32)
    hits_here = jnp.sum(local_hits, axis=2).astype(jnp.bfloat16)
    prior_here = jnp.einsum("ab,pbx->pax", lower, hits_here, preferred_element_type=jnp.float32)
    placing_here = (
        hits_here.astype(jnp.float32)[:, :, :, None]
        * (prior_here[:, :, :, None] == slot_ids[None, None, None, :]).astype(jnp.float32)
    ).astype(jnp.bfloat16)
    sources = all_normed.reshape(peer_count, tok_rows, all_normed.shape[1])
    incoming = jnp.einsum(
        "ptxc,ptd->pxcd", placing_here, sources, preferred_element_type=jnp.float32
    ).astype(jnp.bfloat16)
    returned = serve_rows(
        incoming.reshape(peer_count * local_count, capacity, all_normed.shape[1]),
        w_gate,
        w_up,
        w_down,
    )
    weight_high = gate_table.astype(jnp.bfloat16)
    weight_low = (gate_table - weight_high.astype(jnp.float32)).astype(jnp.bfloat16)
    routed = jnp.einsum("tec,ecd->td", weight_high, returned, preferred_element_type=jnp.float32)
    routed = routed + jnp.einsum(
        "tec,ecd->td", weight_low, returned, preferred_element_type=jnp.float32
    )
    shared = shared_branch(normed, shared_gate, shared_up, shared_down)
    return (routed + shared).astype(jnp.bfloat16)


PLACE = {1: 0, 7: 1, 2: 2, 6: 3, 3: 4, 5: 5, 0: 6, 4: 7}
OWN = PLACE[0]
KEYS = (
    ["M4", "N4"]
    + [way + str(k) + part for way, first in (("M", 1), ("N", 5)) for k in range(first, first + 3)
       for part in ("l", "h")]
    + ["mM1", "mM2", "mM3", "mM4", "mN7", "mN6", "mN5"]
    + ["S%d" % k for k in range(8)]
    + ["mS%d" % k for k in range(8)]
    + ["P%d" % k for k in range(8)]
    + ["u4", "d4"]
    + [way + str(k) + part for way, first in (("u", 1), ("d", 5)) for k in range(first, first + 3)
       for part in ("l", "h")]
)


def fused_kernel(
    sizes, stream, gain, meta_in, wg_hbm, wu_hbm, wd_hbm, sg_hbm, su_hbm, sd_hbm, out,
    tok0, tok1, meta, pair_in, flow_in, wg, wu, wd, inc, slot_gate, place, shared,
    send_sem, recv_sem, load_sem,
):
    n, local_count, capacity, top = sizes
    rows, width = stream.shape
    half = rows // 2
    me = lax.axis_index("ep")
    depth = n // 4
    chips = 2 * depth
    z, y, core = me // 4, (me // 2) % 2, me % 2
    spot = z + y * (chips - 1 - 2 * z)

    def at(where, cc):
        where = lax.rem(where, chips)
        yy = where // depth
        zz = where + yy * (chips - 1 - 2 * where)
        return zz * 4 + yy * 2 + cc

    up, down, sibling = at(spot + 1, core), at(spot + chips - 1, core), at(spot, 1 - core)

    barrier = pltpu.get_barrier_semaphore()
    for peer in (up, down, sibling):
        pl.semaphore_signal(
            barrier, inc=1, device_id={"ep": peer}, device_id_type=pl.DeviceIdType.MESH
        )

    loads = [
        pltpu.make_async_copy(src, dst, load_sem.at[i])
        for i, (src, dst) in enumerate(
            [
                (sg_hbm, wg.at[1]), (su_hbm, wu.at[1]), (sd_hbm, wd.at[1]),
                (wg_hbm.at[0], wg.at[0]), (wu_hbm.at[0], wu.at[0]), (wd_hbm.at[0], wd.at[0]),
                (wg_hbm.at[1], wg.at[1]), (wu_hbm.at[1], wu.at[1]), (wd_hbm.at[1], wd.at[1]),
            ]
        )
    ]
    for load in loads[:6]:
        load.start()

    low, high = pl.ds(0, half), pl.ds(half, half)

    def tok(k):
        return tok0.at[PLACE[k]]

    def own_part(k):
        return tok0.at[PLACE[k] + (8 if PLACE[k] < 6 else 0)]

    routes = {
        "M4": (tok(3).at[low], tok(4).at[low], down),
        "N4": (tok(5).at[high], tok(4).at[high], up),
        "mM4": (meta.at[PLACE[3], 0], meta.at[PLACE[4], 0], down),
        "u4": (own_part(4).at[high], flow_in.at[3, high], up),
        "d4": (own_part(4).at[low], flow_in.at[4, low], down),
    }
    for k in (1, 2, 3):
        routes["mM%d" % k] = (meta.at[PLACE[k - 1], 0], meta.at[PLACE[k], 0], down)
        behind = (9 - k) % 8
        routes["mN%d" % (8 - k)] = (meta.at[PLACE[behind], 0], meta.at[PLACE[8 - k], 0], up)
        for name, rows_of in (("l", low), ("h", high)):
            routes["M%d%s" % (k, name)] = (tok(k - 1).at[rows_of], tok(k).at[rows_of], down)
            routes["N%d%s" % (8 - k, name)] = (tok(behind).at[rows_of], tok(8 - k).at[rows_of], up)
            routes["u%d%s" % (k, name)] = (
                own_part(k).at[rows_of], flow_in.at[k - 1, rows_of], up
            )
            routes["d%d%s" % (8 - k, name)] = (
                own_part(8 - k).at[rows_of], flow_in.at[8 - k, rows_of], down
            )
    for k in range(8):
        s = PLACE[k]
        routes["S%d" % k] = (tok0.at[s], tok1.at[s], sibling)
        routes["mS%d" % k] = (meta.at[s, 0], meta.at[s, 1], sibling)
        routes["P%d" % k] = (tok1.at[s], pair_in.at[s], sibling)

    def copy_of(key):
        src, dst, peer = routes[key]
        i = KEYS.index(key)
        return pltpu.make_async_remote_copy(
            src_ref=src, dst_ref=dst, send_sem=send_sem.at[i], recv_sem=recv_sem.at[i],
            device_id={"ep": peer}, device_id_type=pl.DeviceIdType.MESH,
        )

    def send(*keys):
        for key in keys:
            copy_of(key).start()

    def arrived(*keys):
        for key in keys:
            copy_of(key).wait_recv()

    def sent(*keys):
        for key in keys:
            copy_of(key).wait_send()

    piece = 32

    def norm_rows(i, carry):
        span = pl.ds(pl.multiple_of(i * piece, piece), piece)
        wide = stream[span, :].astype(jnp.float32)
        mean = jnp.mean(wide, axis=-1, keepdims=True)
        centred = wide - mean
        var = jnp.mean(centred * centred, axis=-1, keepdims=True)
        tok0[OWN, span, :] = (centred * lax.rsqrt(var + 1e-05) * gain[...]).astype(jnp.bfloat16)
        return carry

    lax.fori_loop(0, rows // piece, norm_rows, 0)
    meta[OWN, 0] = meta_in[...]
    pl.semaphore_wait(barrier, 3)
    send("mM1", "mN7", "mS0", "M1l", "N7h", "M1h", "N7l", "S0")

    def hidden_of(x, slot):
        gate = jnp.dot(x, wg[slot], preferred_element_type=jnp.float32)
        up = jnp.dot(x, wu[slot], preferred_element_type=jnp.float32)
        return jax.nn.silu(gate) * up

    cols = width // 4

    for load in loads[:3]:
        load.wait()
    hidden = hidden_of(tok0[OWN], 1).astype(jnp.bfloat16)
    for c in range(4):
        part = pl.ds(c * cols, cols)
        shared[:, part] = jnp.dot(hidden, wd[1, :, part], preferred_element_type=jnp.float32)
    for load in loads[6:]:
        load.start()

    first = (me * local_count).astype(jnp.float32)
    tri = (
        lax.broadcasted_iota(jnp.int32, (rows, rows), 0)
        < lax.broadcasted_iota(jnp.int32, (rows, rows), 1)
    ).astype(jnp.float32).astype(jnp.bfloat16)
    slots = local_count * capacity
    slot_row = lax.broadcasted_iota(jnp.int32, (slots, rows), 0).astype(jnp.float32)
    stack_row = lax.broadcasted_iota(jnp.int32, (8, rows), 0)

    def serve_group(base):
        stacked = jnp.zeros((8, rows), jnp.float32)
        gate_rows, hit_rows = [], []
        for k in range(4):
            m = meta[base + k // 2, k % 2]
            ids, weights = m[0:top], m[top:2 * top]
            for x in range(local_count):
                match = (ids == first + x).astype(jnp.float32)
                hit = jnp.sum(match, axis=0, keepdims=True)
                hit_rows.append(hit)
                gate_rows.append(jnp.sum(match * weights, axis=0, keepdims=True))
                stacked = jnp.where(stack_row == k * local_count + x, hit, stacked)
        prior = jnp.dot(stacked.astype(jnp.bfloat16), tri, preferred_element_type=jnp.float32)
        for k in range(4):
            j, r = k // 2, k % 2
            chosen = jnp.zeros((slots, rows), jnp.float32)
            weighted = jnp.zeros((slots, rows), jnp.float32)
            for x in range(local_count):
                q = k * local_count + x
                row = jnp.where(hit_rows[q] > 0, prior[q:q + 1] + x * capacity, -1.0)
                same = (slot_row == row).astype(jnp.float32)
                chosen = chosen + same
                weighted = weighted + same * gate_rows[q]
            slot_gate[k] = jnp.broadcast_to(jnp.sum(weighted, axis=1, keepdims=True), (slots, 128))
            place[k] = chosen.astype(jnp.bfloat16)
            source = tok0 if r == 0 else tok1
            for c in range(4):
                part = pl.ds(c * cols, cols)
                inc[k, :, part] = jnp.dot(
                    place[k], source[base + j, :, part], preferred_element_type=jnp.float32
                ).astype(jnp.bfloat16)
        for x in range(local_count):
            mine = pl.ds(x * capacity, capacity)
            taken = inc[:, mine, :].reshape(4 * capacity, width)
            scale = slot_gate[:, mine, :].reshape(4 * capacity, 128)[:, 0:1]
            act = (hidden_of(taken, x) * scale).astype(jnp.bfloat16)
            for c in range(4):
                part = pl.ds(c * cols, cols)
                made = jnp.dot(act, wd[x, :, part], preferred_element_type=jnp.float32)
                inc[:, mine, part] = made.astype(jnp.bfloat16).reshape(4, capacity, cols)

    def combine_group(base, g):
        for k in range(4):
            j, r = k // 2, k % 2
            for c in range(4):
                part = pl.ds(c * cols, cols)
                total = lax.dot_general(
                    place[k], inc[k, :, part], (((0,), (0,)), ((), ())),
                    preferred_element_type=jnp.float32,
                ).astype(jnp.bfloat16)
                if r == 0:
                    tok0[base + j + 8 * (1 - g // 3), :, part] = total
                else:
                    tok1[base + j, :, part] = total

    def add_into(dst, others, begin, count):
        def step(i, carry):
            span = pl.ds(pl.multiple_of(begin + i * piece, piece), piece)
            total = dst[span, :].astype(jnp.float32)
            for other, offset in others:
                there = pl.ds(pl.multiple_of(begin - offset + i * piece, piece), piece)
                total = total + other[there, :].astype(jnp.float32)
            dst[span, :] = total.astype(jnp.bfloat16)
            return carry

        lax.fori_loop(0, count // piece, step, 0)

    def pair(k):
        return (pair_in.at[PLACE[k]], 0)

    def group(g, carry):
        @pl.when(g == 0)
        def _():
            arrived("mM1", "mN7")
            send("mM2", "mN6", "mS1", "mS7")
            arrived("M1l")
            send("M2l")
            arrived("N7h")
            send("N6h")
            arrived("M1h")
            send("M2h")
            arrived("N7l")
            send("N6l", "S1", "S7")
            for load in loads[3:]:
                load.wait()
            arrived("S1", "S7", "mS1", "mS7")

        @pl.when(g == 1)
        def _():
            arrived("mM2", "mN6")
            send("mM3", "mN5", "mS2", "mS6")
            arrived("M2l")
            send("M3l")
            arrived("N6h")
            send("N5h")
            arrived("M2h")
            send("M3h")
            arrived("N6l")
            send("N5l", "S2", "S6")
            arrived("S2", "S6", "mS2", "mS6")

        @pl.when(g == 2)
        def _():
            arrived("mM3", "mN5")
            send("mM4", "mS3", "mS5")
            arrived("M3l")
            send("M4")
            arrived("N5h")
            send("N4")
            arrived("M3h", "N5l")
            send("S3", "S5")
            arrived("S3", "S5", "mS3", "mS5")

        @pl.when(g == 3)
        def _():
            arrived("mM4", "M4", "N4")
            send("mS4", "S4")
            arrived("S0", "mS0", "S4", "mS4")

        base = 2 * g
        serve_group(base)

        @pl.when(g == 3)
        def _():
            sent("S0", "S4", "M1l", "M1h", "N7l", "N7h")

        combine_group(base, g)

        @pl.when(g == 0)
        def _():
            send("P1", "P7")

        @pl.when(g == 1)
        def _():
            send("P2", "P6")

        @pl.when(g == 2)
        def _():
            send("P3", "P5")
            arrived("P3")
            add_into(own_part(3), [pair(3)], 0, half)
            send("u3l")
            arrived("P5")
            add_into(own_part(5), [pair(5)], half, half)
            send("d5h")

        @pl.when(g == 3)
        def _():
            send("P4", "P0")

        return carry

    lax.fori_loop(0, 4, group, 0)
    arrived("P4")
    add_into(own_part(4), [pair(4)], half, half)
    send("u4")
    add_into(own_part(4), [pair(4)], 0, half)
    send("d4")
    arrived("P0", "P1", "P2", "P6", "P7")

    def pass_on(key, dst, k, landing, begin):
        arrived(key)
        add_into(dst, [pair(k), (flow_in.at[landing], 0)], begin, half)

    pass_on("u4", own_part(3), 3, 3, half)
    send("u3h")
    pass_on("d4", own_part(5), 5, 4, 0)
    send("d5l")
    for k in (2, 1):
        for name, begin in (("l", 0), ("h", half)):
            other = "h" if name == "l" else "l"
            pass_on("u%d%s" % (k + 1, name), own_part(k), k, k, begin)
            send("u%d%s" % (k, name))
            pass_on("d%d%s" % (7 - k, other), own_part(8 - k), 8 - k, 7 - k, half - begin)
            send("d%d%s" % (8 - k, other))
    arrived("u1l", "u1h", "d7l", "d7h")

    def finish(i, carry):
        span = pl.ds(pl.multiple_of(i * piece, piece), piece)
        total = shared[span, :] + tok0[OWN, span, :].astype(jnp.float32)
        for other in (pair_in.at[OWN], flow_in.at[0], flow_in.at[7]):
            total = total + other[span, :].astype(jnp.float32)
        out[span, :] = total.astype(jnp.bfloat16)
        return carry

    lax.fori_loop(0, rows // piece, finish, 0)
    waited = ("S0", "S4", "M1l", "M1h", "N7l", "N7h")
    sent(*[key for key in KEYS if key not in waited])


def fused_device(
    stream, norm_gain, routing, gates, w_gate, w_up, w_down, shared_gate, shared_up, shared_down
):
    rows, width = stream.shape
    top = routing.shape[1]
    local_count, _, hidden = w_gate.shape
    n = lax.axis_size("ep")
    capacity = 2 * rows * top // (local_count * n)
    slots = local_count * capacity
    meta = jnp.concatenate([routing.astype(jnp.float32), gates], axis=1).T
    bf16, f32 = jnp.bfloat16, jnp.float32
    vmem, anywhere = pl.BlockSpec(memory_space=pltpu.VMEM), pl.BlockSpec(memory_space=pl.ANY)
    return pl.pallas_call(
        functools.partial(fused_kernel, (n, local_count, capacity, top)),
        out_shape=jax.ShapeDtypeStruct((rows, width), bf16),
        in_specs=[vmem] * 3 + [anywhere] * 6,
        out_specs=vmem,
        scratch_shapes=[
            pltpu.VMEM((14, rows, width), bf16),
            pltpu.VMEM((8, rows, width), bf16),
            pltpu.VMEM((8, 2, 2 * top, rows), f32),
            pltpu.VMEM((8, rows, width), bf16),
            pltpu.VMEM((8, rows, width), bf16),
            pltpu.VMEM((2, width, hidden), bf16),
            pltpu.VMEM((2, width, hidden), bf16),
            pltpu.VMEM((2, hidden, width), bf16),
            pltpu.VMEM((4, slots, width), bf16),
            pltpu.VMEM((4, slots, 128), f32),
            pltpu.VMEM((4, slots, rows), bf16),
            pltpu.VMEM((rows, width), f32),
            pltpu.SemaphoreType.DMA((len(KEYS),)),
            pltpu.SemaphoreType.DMA((len(KEYS),)),
            pltpu.SemaphoreType.DMA((9,)),
        ],
        compiler_params=pltpu.CompilerParams(
            collective_id=0, has_side_effects=True, vmem_limit_bytes=63 * 1024 * 1024
        ),
    )(stream, norm_gain.reshape(1, -1), meta, w_gate, w_up, w_down, shared_gate, shared_up, shared_down)


def on_device(stream, norm_gain, routing, gates, w_gate, *rest):
    ring = lax.axis_size("ep") // 4
    fits = ring == 4 and w_gate.shape[0] == 2 and rest[2].shape == w_gate.shape[1:]
    run = fused_device if fits else generic_device
    return run(stream, norm_gain, routing, gates, w_gate, *rest)


def solution(mesh):
    placed = (
        P(("grp", "ep"), None),
        P(),
        P(("grp", "ep"), None),
        P(("grp", "ep"), None),
        P("ep", None, None),
        P("ep", None, None),
        P("ep", None, None),
        P(),
        P(),
        P(),
    )
    return jax.shard_map(
        on_device, mesh=mesh, in_specs=placed, out_specs=P(("grp", "ep"), None), check_vma=False
    )
```

profile of v0, /device:TPU:8, one launch (start us, length us, event | category | flops | bytes accessed | tf_op | source)
XLA Modules:
  0.0 175.8 jit_solution(10561745799029415599)
XLA Ops:
  0.0 0.7 convert_element_type.3
  0.7 1.3 maximum_bitcast_fusion.meta_in
  2.0 171.5 %shard_map.100 = bf16[256,2048]{1,0:T(8,128)(2,1)} custom-call(bf16[256,2048]{1,0:T(8,128)(2,1)} %stream.1, f32[1,2048]{1,0:T(1,128)} %bitcast.3, f32[8,256]{1,0:T(8,128)} %maximum_bitcast_fusion.meta_in, bf16[2,2048,512]{2,1,0:T(8,128)(2,1)} %wg_hbm.1, bf16[2,2048,512]{2,1,0:T(8,128)(2,1)} %wu_hbm.1, bf16[2,512,2048]{2,1,0:T(8,128)(2,1)} %wd_hbm.1, ...), custom_call_target="tpu_custom_call" | custom-call | tf_op jit(solution)/shard_map/pallas_call | solution.py:448
  173.5 2.3 %copy.12 = bf16[256,2048]{1,0:T(8,128)(2,1)} copy(bf16[256,2048]{1,0:T(8,128)(2,1)} %shard_map.100) | data formatting | bytes 2097152
where the time goes:
time: 178 us; the launch traced here: 176 us
  Pallas kernels  171 us (96%)
  local copies, waits for them, and re-layouts  2.3 us (1%)
  other arithmetic  1.98 us (1%)
    pallas_call x1, Pallas kernels, fused_device(): pl.pallas_call(functools.partial(fused_kernel, (n, local_count, capacity,...  171 us

commit v1 on v0

v1 whole, which is shorter than its diff:
```python
import functools
import jax
import jax.numpy as jnp
from jax import lax
from jax.experimental import pallas as pl
from jax.experimental.pallas import tpu as pltpu
from jax.sharding import PartitionSpec as P


def layer_norm(stream, norm_gain):
    widened = stream.astype(jnp.float32)
    row_mean = jnp.mean(widened, axis=-1, keepdims=True)
    variance = jnp.mean(jnp.square(widened - row_mean), axis=-1, keepdims=True)
    return ((widened - row_mean) * lax.rsqrt(variance + 1e-05) * norm_gain).astype(jnp.bfloat16)


def shared_branch(normed, shared_gate, shared_up, shared_down):
    shared_hidden = (
        jax.nn.silu(jnp.dot(normed, shared_gate, preferred_element_type=jnp.float32))
        * jnp.dot(normed, shared_up, preferred_element_type=jnp.float32)
    ).astype(jnp.bfloat16)
    return jnp.dot(shared_hidden, shared_down, preferred_element_type=jnp.float32)


def serve_rows(received, w_gate, w_up, w_down):
    local_count = w_gate.shape[0]
    blocks = received.reshape((-1, local_count) + received.shape[1:])
    gate_act = jnp.einsum("sxcd,xdh->sxch", blocks, w_gate, preferred_element_type=jnp.float32)
    up_act = jnp.einsum("sxcd,xdh->sxch", blocks, w_up, preferred_element_type=jnp.float32)
    hidden = (jax.nn.silu(gate_act) * up_act).astype(jnp.bfloat16)
    produced = jnp.einsum(
        "sxch,xhd->sxcd", hidden, w_down, preferred_element_type=jnp.float32
    ).astype(jnp.bfloat16)
    return lax.all_to_all(
        produced.reshape(received.shape), "ep", split_axis=0, concat_axis=0, tiled=True
    )


def generic_device(
    stream, norm_gain, routing, gates, w_gate, w_up, w_down, shared_gate, shared_up, shared_down
):
    tok_rows, top_count = routing.shape
    local_count = w_gate.shape[0]
    peer_count = lax.axis_size("ep")
    experts = local_count * peer_count
    capacity = 2 * tok_rows * top_count // experts
    normed = layer_norm(stream, norm_gain)
    row_ids = jnp.arange(tok_rows, dtype=jnp.int32)
    lower = (row_ids[:, None] > row_ids[None, :]).astype(jnp.bfloat16)
    slot_ids = jnp.arange(capacity, dtype=jnp.int32).astype(jnp.float32)
    expert_hits = (
        routing[:, :, None] == jnp.arange(experts, dtype=jnp.int32)[None, None, :]
    ).astype(jnp.float32)
    token_hits = jnp.sum(expert_hits, axis=1).astype(jnp.bfloat16)
    earlier = jnp.dot(lower, token_hits, preferred_element_type=jnp.float32)
    slot_index = jnp.sum(earlier[:, None, :] * expert_hits, axis=2)
    slot_hits = (slot_index[:, :, None] == slot_ids[None, None, :]).astype(jnp.float32)
    gate_table = jnp.sum(
        gates[:, :, None, None] * expert_hits[:, :, :, None] * slot_hits[:, :, None, :], axis=1
    )
    all_normed = lax.all_gather(normed, "ep", axis=0, tiled=True)
    all_routing = lax.all_gather(routing, "ep", axis=0, tiled=True)
    first_expert = lax.axis_index("ep") * local_count
    shifted = all_routing.reshape(peer_count, tok_rows, top_count) - first_expert
    local_hits = (
        shifted[:, :, :, None] == jnp.arange(local_count, dtype=jnp.int32)[None, None, None, :]
    ).astype(jnp.float32)
    hits_here = jnp.sum(local_hits, axis=2).astype(jnp.bfloat16)
    prior_here = jnp.einsum("ab,pbx->pax", lower, hits_here, preferred_element_type=jnp.float32)
    placing_here = (
        hits_here.astype(jnp.float32)[:, :, :, None]
        * (prior_here[:, :, :, None] == slot_ids[None, None, None, :]).astype(jnp.float32)
    ).astype(jnp.bfloat16)
    sources = all_normed.reshape(peer_count, tok_rows, all_normed.shape[1])
    incoming = jnp.einsum(
        "ptxc,ptd->pxcd", placing_here, sources, preferred_element_type=jnp.float32
    ).astype(jnp.bfloat16)
    returned = serve_rows(
        incoming.reshape(peer_count * local_count, capacity, all_normed.shape[1]),
        w_gate,
        w_up,
        w_down,
    )
    weight_high = gate_table.astype(jnp.bfloat16)
    weight_low = (gate_table - weight_high.astype(jnp.float32)).astype(jnp.bfloat16)
    routed = jnp.einsum("tec,ecd->td", weight_high, returned, preferred_element_type=jnp.float32)
    routed = routed + jnp.einsum(
        "tec,ecd->td", weight_low, returned, preferred_element_type=jnp.float32
    )
    shared = shared_branch(normed, shared_gate, shared_up, shared_down)
    return (routed + shared).astype(jnp.bfloat16)


CORNER = (
    "gBA0", "gCA1", "gCA2", "gBA1", "gCA3", "xA", "gBC3", "gBA2", "gCB0", "gCB1", "gBC0", "gBC2",
    "gBA3", "gCB2", "xC", "sC", "sA", "rCC1", "gBG1", "gCD2", "xD", "sD", "gBG2", "xB",
    "rCD1", "rBD3", "rBD0", "xH", "sH", "rCC3", "rBH2", "rCH3", "rBH1", "rCH0", "xG", "sG",
    "sB", "gBF3", "rCG0", "gBE0", "rCG1", "rCG3", "rCG2", "rCC0", "gBE1", "rBB3", "xE", "sE",
    "xF", "sF", "rBE3", "rCF2", "rBF1", "rBB2", "rBF0", "rBD2", "rCF3", "rCE1", "rCE2", "fA2",
    "rBB0", "rBB1", "rCE0", "rCC2", "fA0", "fA3", "fA1",
)
MIDDLE = (
    "xC", "gAC3", "gDC3", "gEC3", "gEC1", "gDC0", "gAC2", "gAC0", "gDC1", "gAC1", "sC", "gED3",
    "gEA1", "gDE1", "gEA2", "gAD1", "gDA3", "gDB0", "gAG1", "gEB0", "gAG2", "gEB3", "gEB1", "gDH0",
    "gAH0", "gEB2", "gEC0", "gEC2", "xB", "xA", "sB", "gDH3", "gAH3", "gAG0", "xD", "gAG3",
    "gAF3", "xG", "sG", "sD", "gDE0", "gAE0", "gAE1", "xH", "gDE2", "gAE2", "xE", "sE",
    "sA", "sH", "rEE3", "gAF2", "rAD2", "xF", "sF", "rEH1", "rDA0", "rEH2", "rDF1", "rDG0",
    "rEG1", "rAB1", "rDG3", "rDD1", "rDF0", "rAB2", "rEG2", "rAA1", "rEH0", "rEH3", "rAA2", "rDF2",
    "rAB0", "rEF3", "rDB3", "rEE1", "rDD3", "rDD0", "rEE2", "rAA3", "fC1", "rEE0", "fC3", "fC2",
    "fC0",
)

PLANS = {"A": CORNER, "C": MIDDLE}
PARTS = 4


def across(block):
    return chr(65 + ((ord(block) - 65) ^ 1))


def ahead(block):
    n = ord(block) - 65
    return chr(65 + (3 - n // 2) * 2 + n % 2)


def seen_from(role, to, block):
    if to in ("A", "C"):
        return to, block
    if to in ("B", "D"):
        return role, across(block)
    return role, ahead(block)


SLOT = {role: {s[1]: i for i, s in enumerate([s for s in plan if s[0] == "s"])} for role, plan in PLANS.items()}
LANDING = {"A": {}, "C": {}}
for _role, _plan in PLANS.items():
    for _step in _plan:
        if _step[0] == "r":
            _there, _name = seen_from(_role, _step[1], _step[2])
            LANDING[_there][(_name, _step[3], _role, _step[1])] = len(LANDING[_there])
LANDINGS = max(len(v) for v in LANDING.values())
SENDS = 24 + max(sum(2 if s[0] == "g" else 1 for s in plan) for plan in PLANS.values())
R_META, R_SIB, R_SIBMETA, R_PAIR, R_LAND = 8 * PARTS, 8 * PARTS + 8, 8 * PARTS + 16, 8 * PARTS + 24, 8 * PARTS + 32


def fused_kernel(
    sizes, stream, gain, meta_in, wg_hbm, wu_hbm, wd_hbm, sg_hbm, su_hbm, sd_hbm, out,
    tok0, tok1, mine, meta, pair_in, flow_in, wg, wu, wd, inc, slot_gate, place, shared,
    send_sem, recv_sem, load_sem,
):
    n, local_count, capacity, top = sizes
    rows, width = stream.shape
    part_rows = rows // PARTS
    me = lax.axis_index("ep")
    z, y, core = me // 4, (me // 2) % 2, me % 2
    z_next = z + 1 - 2 * (z % 2)
    is_corner = z * (3 - z) == 0
    peers = {
        "A": z_next * 4 + y * 2 + core,
        "C": z_next * 4 + y * 2 + core,
        "B": z * 4 + (1 - y) * 2 + core,
        "D": z * 4 + (1 - y) * 2 + core,
        "E": (3 - z) * 4 + y * 2 + core,
    }
    sibling = z * 4 + y * 2 + 1 - core

    def when_role(role):
        return pl.when(is_corner if role == "A" else jnp.logical_not(is_corner))

    barrier = pltpu.get_barrier_semaphore()

    def greet(who):
        pl.semaphore_signal(
            barrier, inc=1, device_id={"ep": who}, device_id_type=pl.DeviceIdType.MESH
        )

    greet(sibling)
    greet(peers["A"])
    greet(peers["B"])

    @when_role("C")
    def _():
        greet(peers["E"])

    loads = [
        pltpu.make_async_copy(src, dst, load_sem.at[i])
        for i, (src, dst) in enumerate(
            [
                (sg_hbm, wg.at[1]), (su_hbm, wu.at[1]), (sd_hbm, wd.at[1]),
                (wg_hbm.at[0], wg.at[0]), (wu_hbm.at[0], wu.at[0]), (wd_hbm.at[0], wd.at[0]),
                (wg_hbm.at[1], wg.at[1]), (wu_hbm.at[1], wu.at[1]), (wd_hbm.at[1], wd.at[1]),
            ]
        )
    ]
    for load in loads[:6]:
        load.start()

    def remote(src, dst, send, recv, peer):
        return pltpu.make_async_remote_copy(
            src_ref=src, dst_ref=dst, send_sem=send_sem.at[send], recv_sem=recv_sem.at[recv],
            device_id={"ep": peer}, device_id_type=pl.DeviceIdType.MESH,
        )

    def span_of(part):
        return pl.ds(int(part) * part_rows, part_rows)

    def sibling_copies(slot):
        return (
            remote(meta.at[slot, 0], meta.at[slot, 1], slot, R_SIBMETA + slot, sibling),
            remote(tok0.at[slot], tok1.at[slot], 8 + slot, R_SIB + slot, sibling),
        )

    def pair_copy(slot):
        return remote(tok1.at[slot], pair_in.at[slot], 16 + slot, R_PAIR + slot, sibling)

    piece = 16

    def add_rows(dst, begin, count, others, onto=None):
        def step(i, carry):
            offset = pl.multiple_of(i * piece, piece)
            span = pl.ds(begin + offset, piece)
            total = dst[span, :].astype(jnp.float32)
            for other, start in others:
                total = total + other[pl.ds(start + offset, piece), :].astype(jnp.float32)
            if onto is None:
                dst[span, :] = total.astype(jnp.bfloat16)
            else:
                out[span, :] = (total + onto[span, :]).astype(jnp.bfloat16)
            return carry

        lax.fori_loop(0, count // piece, step, 0)

    class Walk:
        def __init__(self, role):
            self.role, self.own, self.slots = role, role, SLOT[role]
            self.waited, self.used, self.copies = set(), 24, []

        def arrived(self, src, recv, key):
            if key not in self.waited:
                self.waited.add(key)
                remote(src, src, 0, recv, sibling).wait_recv()

        def tokens(self, block, part):
            slot = self.slots[block]
            if block != self.own:
                self.arrived(tok0.at[slot, span_of(part)], slot * PARTS + int(part), ("t", block, part))

        def details(self, block):
            slot = self.slots[block]
            if block != self.own:
                self.arrived(meta.at[slot, 0], R_META + slot, ("m", block))

        def push(self, views, recv, to):
            send, self.used = self.used, self.used + 1

            def copy():
                src, dst = views()
                return remote(src, dst, send, recv, peers[to])

            self.copies.append(copy)
            copy().start()

        def summed(self, block, part, last=False):
            slot, span = self.slots[block], span_of(part)
            others = []
            self.arrived(pair_in.at[slot], R_PAIR + slot, ("p", block))
            others.append((pair_in.at[slot], int(part) * part_rows))
            for (name, which, _, _), k in LANDING[self.role].items():
                if (name, which) == (block, part):
                    self.arrived(flow_in.at[k], R_LAND + k, ("l", k))
                    others.append((flow_in.at[k], 0))
            add_rows(mine.at[slot], int(part) * part_rows, part_rows, others, shared if last else None)

        def run(self, step):
            if step[0] == "g":
                to, block, part = step[1:]
                there, name = seen_from(self.role, to, block)
                slot, target = self.slots[block], SLOT[there][name]
                if part == "0":
                    self.details(block)
                    self.push(lambda: (meta.at[slot, 0], meta.at[target, 0]), R_META + target, to)
                self.tokens(block, part)
                self.push(
                    lambda: (tok0.at[slot, span_of(part)], tok0.at[target, span_of(part)]),
                    target * PARTS + int(part), to,
                )
            elif step[0] == "x":
                block = step[1]
                self.details(block)
                for part in range(PARTS):
                    self.tokens(block, str(part))
                for copy in sibling_copies(self.slots[block]):
                    copy.start()
            elif step[0] == "r":
                to, block, part = step[1:]
                there, name = seen_from(self.role, to, block)
                self.summed(block, part)
                k = LANDING[there][(name, part, self.role, to)]
                slot = self.slots[block]
                self.push(lambda: (mine.at[slot, span_of(part)], flow_in.at[k]), R_LAND + k, to)
            elif step[0] == "f":
                self.summed(step[1], step[2], last=True)

    walks = {role: Walk(role) for role in PLANS}
    segments = {}
    for role, plan in PLANS.items():
        parts = [[]]
        for step in plan:
            if step[0] == "s":
                parts.append([])
            else:
                parts[-1].append(step)
        own_first = [s for s in parts[0] if s[0] in "gx" and s[1 + (s[0] == "g")] == role]
        segments[role] = [own_first, [s for s in parts[0] if s not in own_first]] + parts[1:]

    def run_segment(role, i):
        for step in segments[role][i]:
            walks[role].run(step)

    norm_piece = 32

    def norm_into(slot):
        def norm_rows(i, carry):
            span = pl.ds(pl.multiple_of(i * norm_piece, norm_piece), norm_piece)
            wide = stream[span, :].astype(jnp.float32)
            mean = jnp.mean(wide, axis=-1, keepdims=True)
            centred = wide - mean
            var = jnp.mean(centred * centred, axis=-1, keepdims=True)
            tok0[slot, span, :] = (centred * lax.rsqrt(var + 1e-05) * gain[...]).astype(jnp.bfloat16)
            return carry

        lax.fori_loop(0, rows // norm_piece, norm_rows, 0)
        meta[slot, 0] = meta_in[...]

    own_slot = lax.select(is_corner, SLOT["A"]["A"], SLOT["C"]["C"])
    norm_into(own_slot)

    @when_role("A")
    def _():
        pl.semaphore_wait(barrier, 3)
        run_segment("A", 0)

    @when_role("C")
    def _():
        pl.semaphore_wait(barrier, 4)
        run_segment("C", 0)

    def hidden_of(x, slot):
        gate = jnp.dot(x, wg[slot], preferred_element_type=jnp.float32)
        up = jnp.dot(x, wu[slot], preferred_element_type=jnp.float32)
        return jax.nn.silu(gate) * up

    cols = width // 4

    for load in loads[:3]:
        load.wait()
    hidden = hidden_of(tok0[own_slot], 1).astype(jnp.bfloat16)
    for c in range(4):
        part = pl.ds(c * cols, cols)
        shared[:, part] = jnp.dot(hidden, wd[1, :, part], preferred_element_type=jnp.float32)
    for load in loads[6:]:
        load.start()

    first = (me * local_count).astype(jnp.float32)
    tri = (
        lax.broadcasted_iota(jnp.int32, (rows, rows), 0)
        < lax.broadcasted_iota(jnp.int32, (rows, rows), 1)
    ).astype(jnp.float32).astype(jnp.bfloat16)
    slots = local_count * capacity
    slot_row = lax.broadcasted_iota(jnp.int32, (slots, rows), 0).astype(jnp.float32)
    stack_row = lax.broadcasted_iota(jnp.int32, (8, rows), 0)

    def serve(g):
        stacked = jnp.zeros((8, rows), jnp.float32)
        gate_rows, hit_rows = [], []
        for r in range(2):
            m = meta[g, r]
            ids, weights = m[0:top], m[top:2 * top]
            for x in range(local_count):
                match = (ids == first + x).astype(jnp.float32)
                hit = jnp.sum(match, axis=0, keepdims=True)
                hit_rows.append(hit)
                gate_rows.append(jnp.sum(match * weights, axis=0, keepdims=True))
                stacked = jnp.where(stack_row == r * local_count + x, hit, stacked)
        prior = jnp.dot(stacked.astype(jnp.bfloat16), tri, preferred_element_type=jnp.float32)
        for r in range(2):
            chosen = jnp.zeros((slots, rows), jnp.float32)
            weighted = jnp.zeros((slots, rows), jnp.float32)
            for x in range(local_count):
                q = r * local_count + x
                row = jnp.where(hit_rows[q] > 0, prior[q:q + 1] + x * capacity, -1.0)
                same = (slot_row == row).astype(jnp.float32)
                chosen = chosen + same
                weighted = weighted + same * gate_rows[q]
            slot_gate[r] = jnp.broadcast_to(jnp.sum(weighted, axis=1, keepdims=True), (slots, 128))
            place[r] = chosen.astype(jnp.bfloat16)
            source = tok0 if r == 0 else tok1
            for c in range(4):
                part = pl.ds(c * cols, cols)
                inc[r, :, part] = jnp.dot(
                    place[r], source[g, :, part], preferred_element_type=jnp.float32
                ).astype(jnp.bfloat16)
        for x in range(local_count):
            held = pl.ds(x * capacity, capacity)
            taken = inc[:, held, :].reshape(2 * capacity, width)
            scale = slot_gate[:, held, :].reshape(2 * capacity, 128)[:, 0:1]
            act = (hidden_of(taken, x) * scale).astype(jnp.bfloat16)
            for c in range(4):
                part = pl.ds(c * cols, cols)
                made = jnp.dot(act, wd[x, :, part], preferred_element_type=jnp.float32)
                inc[:, held, part] = made.astype(jnp.bfloat16).reshape(2, capacity, cols)
        for r in (1, 0):
            for c in range(4):
                part = pl.ds(c * cols, cols)
                total = lax.dot_general(
                    place[r], inc[r, :, part], (((0,), (0,)), ((), ())),
                    preferred_element_type=jnp.float32,
                ).astype(jnp.bfloat16)
                if r == 0:
                    mine[g, :, part] = total
                else:
                    tok1[g, :, part] = total
            if r == 1:
                pair_copy(g).start()

    def block(g, carry):
        for i in range(8):
            for role in PLANS:
                @pl.when((g == i) & (is_corner if role == "A" else jnp.logical_not(is_corner)))
                def _():
                    run_segment(role, i + 1)

        @pl.when(g == 0)
        def _():
            for load in loads[3:]:
                load.wait()

        for copy in sibling_copies(g):
            copy.wait_recv()
        serve(g)
        return carry

    lax.fori_loop(0, 8, block, 0)

    for role in PLANS:
        @when_role(role)
        def _():
            run_segment(role, 9)
            for copy in walks[role].copies:
                copy().wait_send()

    def drain(g, carry):
        for copy in sibling_copies(g) + (pair_copy(g),):
            copy.wait_send()
        return carry

    lax.fori_loop(0, 8, drain, 0)


def fused_device(
    stream, norm_gain, routing, gates, w_gate, w_up, w_down, shared_gate, shared_up, shared_down
):
    rows, width = stream.shape
    top = routing.shape[1]
    local_count, _, hidden = w_gate.shape
    n = lax.axis_size("ep")
    capacity = 2 * rows * top // (local_count * n)
    slots = local_count * capacity
    meta = jnp.concatenate([routing.astype(jnp.float32), gates], axis=1).T
    bf16, f32 = jnp.bfloat16, jnp.float32
    vmem, anywhere = pl.BlockSpec(memory_space=pltpu.VMEM), pl.BlockSpec(memory_space=pl.ANY)
    return pl.pallas_call(
        functools.partial(fused_kernel, (n, local_count, capacity, top)),
        out_shape=jax.ShapeDtypeStruct((rows, width), bf16),
        in_specs=[vmem] * 3 + [anywhere] * 6,
        out_specs=vmem,
        scratch_shapes=[
            pltpu.VMEM((8, rows, width), bf16),
            pltpu.VMEM((8, rows, width), bf16),
            pltpu.VMEM((8, rows, width), bf16),
            pltpu.VMEM((8, 2, 2 * top, rows), f32),
            pltpu.VMEM((8, rows, width), bf16),
            pltpu.VMEM((LANDINGS, rows // PARTS, width), bf16),
            pltpu.VMEM((2, width, hidden), bf16),
            pltpu.VMEM((2, width, hidden), bf16),
            pltpu.VMEM((2, hidden, width), bf16),
            pltpu.VMEM((2, slots, width), bf16),
            pltpu.VMEM((2, slots, 128), f32),
            pltpu.VMEM((2, slots, rows), bf16),
            pltpu.VMEM((rows, width), f32),
            pltpu.SemaphoreType.DMA((SENDS,)),
            pltpu.SemaphoreType.DMA((R_LAND + LANDINGS,)),
            pltpu.SemaphoreType.DMA((9,)),
        ],
        compiler_params=pltpu.CompilerParams(
            collective_id=0, has_side_effects=True, vmem_limit_bytes=63 * 1024 * 1024
        ),
    )(stream, norm_gain.reshape(1, -1), meta, w_gate, w_up, w_down, shared_gate, shared_up, shared_down)


def on_device(stream, norm_gain, routing, gates, w_gate, *rest):
    ring = lax.axis_size("ep") // 4
    fits = ring == 4 and w_gate.shape[0] == 2 and rest[2].shape == w_gate.shape[1:]
    run = fused_device if fits else generic_device
    return run(stream, norm_gain, routing, gates, w_gate, *rest)


def solution(mesh):
    placed = (
        P(("grp", "ep"), None),
        P(),
        P(("grp", "ep"), None),
        P(("grp", "ep"), None),
        P("ep", None, None),
        P("ep", None, None),
        P("ep", None, None),
        P(),
        P(),
        P(),
    )
    return jax.shard_map(
        on_device, mesh=mesh, in_specs=placed, out_specs=P(("grp", "ep"), None), check_vma=False
    )
```

time: 178 us -> 156 us (0.88); the launches traced: 176 us -> 156 us
  Pallas kernels: 171 us -> 151 us
    pallas_call x1, Pallas kernels: 171 us -> 151 us  [fused_device(): pl.pallas_call(functools.partial(fused_kernel, (n, local_count, capacity,...]
where the time goes in v1:
time: 156 us
  Pallas kernels  151 us (97%)
  local copies, waits for them, and re-layouts  2.3 us (1%)
  other arithmetic  1.98 us (1%)
    pallas_call x1, Pallas kernels, fused_device(): pl.pallas_call(functools.partial(fused_kernel, (n, local_count, capacity,...  151 us

profile of v1, /device:TPU:8, one launch (start us, length us, event | category | flops | bytes accessed | tf_op | source)
XLA Modules:
  0.0 155.7 jit_solution(16879389613567665876)
XLA Ops:
  0.0 0.7 convert_element_type.3
  0.7 1.3 maximum_bitcast_fusion.meta_in
  2.0 151.4 %shard_map.100 = bf16[256,2048]{1,0:T(8,128)(2,1)} custom-call(bf16[256,2048]{1,0:T(8,128)(2,1)} %stream.1, f32[1,2048]{1,0:T(1,128)} %bitcast.3, f32[8,256]{1,0:T(8,128)} %maximum_bitcast_fusion.meta_in, bf16[2,2048,512]{2,1,0:T(8,128)(2,1)} %wg_hbm.1, bf16[2,2048,512]{2,1,0:T(8,128)(2,1)} %wu_hbm.1, bf16[2,512,2048]{2,1,0:T(8,128)(2,1)} %wd_hbm.1, ...), custom_call_target="tpu_custom_call" | custom-call | tf_op jit(solution)/shard_map/pallas_call | solution.py:472
  153.4 2.3 %copy.12 = bf16[256,2048]{1,0:T(8,128)(2,1)} copy(bf16[256,2048]{1,0:T(8,128)(2,1)} %shard_map.100) | data formatting | bytes 2097152

commit v2 on v1

--- a/solution.py
+++ b/solution.py
@@ -144,7 +144,7 @@
 
 
 def fused_kernel(
-    sizes, stream, gain, meta_in, wg_hbm, wu_hbm, wd_hbm, sg_hbm, su_hbm, sd_hbm, out,
+    sizes, stream, gain, routing, gates, wg_hbm, wu_hbm, wd_hbm, sg_hbm, su_hbm, sd_hbm, out,
     tok0, tok1, mine, meta, pair_in, flow_in, wg, wu, wd, inc, slot_gate, place, shared,
     send_sem, recv_sem, load_sem,
 ):
@@ -330,7 +330,8 @@
             return carry
 
         lax.fori_loop(0, rows // norm_piece, norm_rows, 0)
-        meta[slot, 0] = meta_in[...]
+        meta[slot, 0, 0:top] = routing[...].astype(jnp.float32)
+        meta[slot, 0, top:2 * top] = gates[...]
 
     own_slot = lax.select(is_corner, SLOT["A"]["A"], SLOT["C"]["C"])
     norm_into(own_slot)
@@ -466,13 +467,12 @@
     n = lax.axis_size("ep")
     capacity = 2 * rows * top // (local_count * n)
     slots = local_count * capacity
-    meta = jnp.concatenate([routing.astype(jnp.float32), gates], axis=1).T
     bf16, f32 = jnp.bfloat16, jnp.float32
     vmem, anywhere = pl.BlockSpec(memory_space=pltpu.VMEM), pl.BlockSpec(memory_space=pl.ANY)
     return pl.pallas_call(
         functools.partial(fused_kernel, (n, local_count, capacity, top)),
-        out_shape=jax.ShapeDtypeStruct((rows, width), bf16),
-        in_specs=[vmem] * 3 + [anywhere] * 6,
+        out_shape=pltpu.VMEM((rows, width), bf16),
+        in_specs=[vmem] * 4 + [anywhere] * 6,
         out_specs=vmem,
         scratch_shapes=[
             pltpu.VMEM((8, rows, width), bf16),
@@ -493,9 +493,12 @@
             pltpu.SemaphoreType.DMA((9,)),
         ],
         compiler_params=pltpu.CompilerParams(
-            collective_id=0, has_side_effects=True, vmem_limit_bytes=63 * 1024 * 1024
+            collective_id=0, has_side_effects=True, vmem_limit_bytes=61 * 1024 * 1024
         ),
-    )(stream, norm_gain.reshape(1, -1), meta, w_gate, w_up, w_down, shared_gate, shared_up, shared_down)
+    )(
+        stream, norm_gain.reshape(1, -1), routing.T, gates.T,
+        w_gate, w_up, w_down, shared_gate, shared_up, shared_down,
+    )
 
 
 def on_device(stream, norm_gain, routing, gates, w_gate, *rest):

time: 156 us -> 152 us (0.974)
  other arithmetic: 1.98 us -> 0 us
where the time goes in v2:
time: 152 us; the launch traced here: 151 us
  Pallas kernels  150 us (99%)
    pallas_call x1, Pallas kernels, fused_device(): pl.pallas_call(functools.partial(fused_kernel, (n, local_count, capacity,...  150 us

profile of v2, /device:TPU:8, one launch (start us, length us, event | category | flops | bytes accessed | tf_op | source)
XLA Modules:
  0.0 151.4 jit_solution(15799378922697157684)
XLA Ops:
  0.0 150.5 %shard_map.100 = bf16[256,2048]{1,0:T(8,128)(2,1)S(1)} custom-call(bf16[256,2048]{1,0:T(8,128)(2,1)} %stream.1, f32[1,2048]{1,0:T(1,128)} %bitcast.3, s32[4,256]{1,0:T(4,128)} %bitcast.4, f32[4,256]{1,0:T(4,128)} %bitcast.5, bf16[2,2048,512]{2,1,0:T(8,128)(2,1)} %wg_hbm.1, bf16[2,2048,512]{2,1,0:T(8,128)(2,1)} %wu_hbm.1, bf16[2,512,2048]{2,1,0:T(8,128)(2,1)} %wd_hbm.1, ...), custom_call_target="tpu_custom_call" | custom-call | tf_op jit(solution)/shard_map/pallas_call | solution.py:472
  150.5 1.0 copy.12

commit v3 on v2

--- a/solution.py
+++ b/solution.py
@@ -92,26 +92,36 @@
 
 
 CORNER = (
-    "gBA0", "gCA1", "gCA2", "gBA1", "gCA3", "xA", "gBC3", "gBA2", "gCB0", "gCB1", "gBC0", "gBC2",
-    "gBA3", "gCB2", "xC", "sC", "sA", "rCC1", "gBG1", "gCD2", "xD", "sD", "gBG2", "xB",
-    "rCD1", "rBD3", "rBD0", "xH", "sH", "rCC3", "rBH2", "rCH3", "rBH1", "rCH0", "xG", "sG",
-    "sB", "gBF3", "rCG0", "gBE0", "rCG1", "rCG3", "rCG2", "rCC0", "gBE1", "rBB3", "xE", "sE",
-    "xF", "sF", "rBE3", "rCF2", "rBF1", "rBB2", "rBF0", "rBD2", "rCF3", "rCE1", "rCE2", "fA2",
-    "rBB0", "rBB1", "rCE0", "rCC2", "fA0", "fA3", "fA1",
+    1104, 1102, 1201, 2000, 1103, 1203, 1204, 1105, 1207, 1125, 1126, 1206, 1215, 1200, 1123, 1202,
+    1120, 1121, 1212, 1205, 1122, 1106, 1101, 2020, 3020, 2030, 1161, 1216, 1230, 1163, 3030, 1162,
+    4227, 1160, 4237, 4234, 4133, 4224, 4132, 3000, 4136, 4131, 4223, 1107, 2070, 1100, 4222, 4226,
+    3070, 4221, 4135, 4277, 4170, 4171, 2060, 4172, 4275, 4276, 1143, 3060, 2010, 4274, 1147, 4260,
+    1146, 4262, 4261, 3010, 4173, 1155, 1154, 4264, 4266, 2050, 4113, 4265, 4263, 4114, 4267, 3050,
+    2040, 4252, 4110, 4251, 4153, 4157, 3040, 4250, 4145, 4156, 4241, 4144, 4243, 4242, 4255, 4111,
+    4116, 4254, 4246, 4115, 4247, 4117, 4130, 4112, 4240, 5004, 4225, 5003, 5001, 5000, 5006, 4220,
+    5007, 5005, 5002,
 )
 MIDDLE = (
-    "xC", "gAC3", "gDC3", "gEC3", "gEC1", "gDC0", "gAC2", "gAC0", "gDC1", "gAC1", "sC", "gED3",
-    "gEA1", "gDE1", "gEA2", "gAD1", "gDA3", "gDB0", "gAG1", "gEB0", "gAG2", "gEB3", "gEB1", "gDH0",
-    "gAH0", "gEB2", "gEC0", "gEC2", "xB", "xA", "sB", "gDH3", "gAH3", "gAG0", "xD", "gAG3",
-    "gAF3", "xG", "sG", "sD", "gDE0", "gAE0", "gAE1", "xH", "gDE2", "gAE2", "xE", "sE",
-    "sA", "sH", "rEE3", "gAF2", "rAD2", "xF", "sF", "rEH1", "rDA0", "rEH2", "rDF1", "rDG0",
-    "rEG1", "rAB1", "rDG3", "rDD1", "rDF0", "rAB2", "rEG2", "rAA1", "rEH0", "rEH3", "rAA2", "rDF2",
-    "rAB0", "rEF3", "rDB3", "rEE1", "rDD3", "rDD0", "rEE2", "rAA3", "fC1", "rEE0", "fC3", "fC2",
-    "fC0",
+    1023, 1025, 1321, 1424, 1323, 1427, 1425, 1324, 1026, 1021, 1020, 1420, 1326, 1401, 1327, 1403,
+    1404, 1027, 1407, 1022, 1024, 1303, 2020, 1406, 1340, 1361, 1037, 1034, 1325, 1402, 1322, 1061,
+    1400, 1367, 1364, 1063, 1422, 1415, 1405, 1300, 1362, 1062, 1366, 1421, 3020, 1307, 1423, 1363,
+    1060, 1435, 2000, 1074, 1077, 1426, 2030, 1410, 2060, 1075, 1076, 1065, 1431, 1067, 1347, 1064,
+    1434, 1066, 1433, 1301, 1043, 1304, 1342, 3030, 3060, 1046, 2070, 1047, 2040, 3000, 4337, 3040,
+    1346, 3070, 1050, 1054, 4373, 1055, 4371, 4372, 1052, 4470, 4445, 4444, 2050, 4336, 1051, 1041,
+    4377, 2010, 4475, 1040, 3050, 1042, 4460, 3010, 4030, 4374, 4453, 4462, 4314, 4376, 4464, 4461,
+    4015, 4317, 4313, 4466, 4310, 4311, 4004, 4463, 4332, 4002, 4467, 4012, 4451, 4352, 4357, 4016,
+    4006, 4003, 4465, 4441, 4001, 4333, 4443, 4000, 4442, 4007, 4356, 4455, 4331, 4350, 4454, 4446,
+    4335, 4005, 5021, 4447, 4334, 5022, 4440, 5023, 5024, 5025, 5027, 5026, 5020,
 )
-
-PLANS = {"A": CORNER, "C": MIDDLE}
-PARTS = 4
+PARTS = 8
+
+
+def step_of(code):
+    kind, to, block, part = "gxsrf"[code // 1000 - 1], "ABCDE"[code // 100 % 10], chr(65 + code // 10 % 10), str(code % 10)
+    return kind + (to if kind in "gr" else "") + block + (part if kind in "grf" else "")
+
+
+PLANS = {"A": [step_of(code) for code in CORNER], "C": [step_of(code) for code in MIDDLE]}
 
 
 def across(block):
@@ -310,8 +320,10 @@
                 parts.append([])
             else:
                 parts[-1].append(step)
-        own_first = [s for s in parts[0] if s[0] in "gx" and s[1 + (s[0] == "g")] == role]
-        segments[role] = [own_first, [s for s in parts[0] if s not in own_first]] + parts[1:]
+        mark = 0
+        while mark < len(parts[0]) and parts[0][mark].rstrip("01234567")[-1] == role and parts[0][mark][0] in "gx":
+            mark += 1
+        segments[role] = [parts[0][:mark], parts[0][mark:]] + parts[1:]
 
     def run_segment(role, i):
         for step in segments[role][i]:

time: 152 us -> 143 us (0.941)
  Pallas kernels: 150 us -> 142 us
    pallas_call x1, Pallas kernels: 150 us -> 142 us  [fused_device(): pl.pallas_call(functools.partial(fused_kernel, (n, local_count, capacity,...]
where the time goes in v3:
time: 143 us
  Pallas kernels  142 us (99%)
    pallas_call x1, Pallas kernels, fused_device(): pl.pallas_call(functools.partial(fused_kernel, (n, local_count, capacity,...  142 us

profile of v3, /device:TPU:8, one launch (start us, length us, event | category | flops | bytes accessed | tf_op | source)
XLA Modules:
  0.0 143.3 jit_solution(1180108046149250444)
XLA Ops:
  0.0 142.3 %shard_map.100 = bf16[256,2048]{1,0:T(8,128)(2,1)S(1)} custom-call(bf16[256,2048]{1,0:T(8,128)(2,1)} %stream.1, f32[1,2048]{1,0:T(1,128)} %bitcast.3, s32[4,256]{1,0:T(4,128)} %bitcast.4, f32[4,256]{1,0:T(4,128)} %bitcast.5, bf16[2,2048,512]{2,1,0:T(8,128)(2,1)} %wg_hbm.1, bf16[2,2048,512]{2,1,0:T(8,128)(2,1)} %wu_hbm.1, bf16[2,512,2048]{2,1,0:T(8,128)(2,1)} %wd_hbm.1, ...), custom_call_target="tpu_custom_call" | custom-call | tf_op jit(solution)/shard_map/pallas_call | solution.py:484
  142.3 1.0 copy.12

commit v4 on v3

--- a/solution.py
+++ b/solution.py
@@ -154,9 +154,9 @@
 
 
 def fused_kernel(
-    sizes, stream, gain, routing, gates, wg_hbm, wu_hbm, wd_hbm, sg_hbm, su_hbm, sd_hbm, out,
+    sizes, stream_hbm, gain, routing, gates, wg_hbm, wu_hbm, wd_hbm, sg_hbm, su_hbm, sd_hbm, out,
     tok0, tok1, mine, meta, pair_in, flow_in, wg, wu, wd, inc, slot_gate, place, shared,
-    send_sem, recv_sem, load_sem,
+    stream, send_sem, recv_sem, load_sem,
 ):
     n, local_count, capacity, top = sizes
     rows, width = stream.shape
@@ -192,6 +192,15 @@
     def _():
         greet(peers["E"])
 
+    rows_in = [
+        pltpu.make_async_copy(
+            stream_hbm.at[pl.ds(p * part_rows, part_rows)], stream.at[pl.ds(p * part_rows, part_rows)],
+            load_sem.at[9 + p],
+        )
+        for p in range(PARTS)
+    ]
+    for copy in rows_in:
+        copy.start()
     loads = [
         pltpu.make_async_copy(src, dst, load_sem.at[i])
         for i, (src, dst) in enumerate(
@@ -329,34 +338,55 @@
         for step in segments[role][i]:
             walks[role].run(step)
 
-    norm_piece = 32
-
-    def norm_into(slot):
-        def norm_rows(i, carry):
-            span = pl.ds(pl.multiple_of(i * norm_piece, norm_piece), norm_piece)
-            wide = stream[span, :].astype(jnp.float32)
-            mean = jnp.mean(wide, axis=-1, keepdims=True)
-            centred = wide - mean
-            var = jnp.mean(centred * centred, axis=-1, keepdims=True)
-            tok0[slot, span, :] = (centred * lax.rsqrt(var + 1e-05) * gain[...]).astype(jnp.bfloat16)
-            return carry
-
-        lax.fori_loop(0, rows // norm_piece, norm_rows, 0)
-        meta[slot, 0, 0:top] = routing[...].astype(jnp.float32)
-        meta[slot, 0, top:2 * top] = gates[...]
+    def norm_part(slot, part):
+        span = pl.ds(pl.multiple_of(part * part_rows, part_rows), part_rows)
+        wide = stream[span, :].astype(jnp.float32)
+        mean = jnp.mean(wide, axis=-1, keepdims=True)
+        centred = wide - mean
+        var = jnp.mean(centred * centred, axis=-1, keepdims=True)
+        tok0[slot, span, :] = (centred * lax.rsqrt(var + 1e-05) * gain[...]).astype(jnp.bfloat16)
 
     own_slot = lax.select(is_corner, SLOT["A"]["A"], SLOT["C"]["C"])
-    norm_into(own_slot)
+    meta[own_slot, 0, 0:top] = routing[...].astype(jnp.float32)
+    meta[own_slot, 0, top:2 * top] = gates[...]
+
+    def begin(role, neighbours):
+        own = SLOT[role][role]
+        steps = sorted(segments[role][0], key=lambda s: s[0] == "x")
+        order = list(dict.fromkeys(int(s[3]) for s in steps if s[0] == "g"))[:2]
+        ready = 0
+        for step in steps:
+            need = 3 if step[0] == "x" or int(step[3]) not in order else order.index(int(step[3])) + 1
+            while ready < need:
+                if ready < len(order):
+                    rows_in[order[ready]].wait()
+                    norm_part(own, order[ready])
+                    if ready == 0:
+                        pl.semaphore_wait(barrier, neighbours)
+                elif ready == 2:
+                    for p in range(PARTS):
+                        if p not in order:
+                            rows_in[p].wait()
+
+                    def norm_rest(p, carry):
+                        @pl.when((p != order[0]) & (p != order[1]))
+                        def _():
+                            norm_part(own, p)
+
+                        return carry
+
+                    lax.fori_loop(0, PARTS, norm_rest, 0)
+                ready += 1
+            walks[role].run(step)
+        assert ready == 3
 
     @when_role("A")
     def _():
-        pl.semaphore_wait(barrier, 3)
-        run_segment("A", 0)
+        begin("A", 3)
 
     @when_role("C")
     def _():
-        pl.semaphore_wait(barrier, 4)
-        run_segment("C", 0)
+        begin("C", 4)
 
     def hidden_of(x, slot):
         gate = jnp.dot(x, wg[slot], preferred_element_type=jnp.float32)
@@ -484,7 +514,7 @@
     return pl.pallas_call(
         functools.partial(fused_kernel, (n, local_count, capacity, top)),
         out_shape=pltpu.VMEM((rows, width), bf16),
-        in_specs=[vmem] * 4 + [anywhere] * 6,
+        in_specs=[anywhere] + [vmem] * 3 + [anywhere] * 6,
         out_specs=vmem,
         scratch_shapes=[
             pltpu.VMEM((8, rows, width), bf16),
@@ -500,9 +530,10 @@
             pltpu.VMEM((2, slots, 128), f32),
             pltpu.VMEM((2, slots, rows), bf16),
             pltpu.VMEM((rows, width), f32),
+            pltpu.VMEM((rows, width), bf16),
             pltpu.SemaphoreType.DMA((SENDS,)),
             pltpu.SemaphoreType.DMA((R_LAND + LANDINGS,)),
-            pltpu.SemaphoreType.DMA((9,)),
+            pltpu.SemaphoreType.DMA((9 + PARTS,)),
         ],
         compiler_params=pltpu.CompilerParams(
             collective_id=0, has_side_effects=True, vmem_limit_bytes=61 * 1024 * 1024

time: 143 us -> 143 us (level)
  no operation moved by 1% of the time
where the time goes in v4:
time: 143 us; the launch traced here: 142 us
  Pallas kernels  141 us (99%)
    pallas_call x1, Pallas kernels, fused_device(): pl.pallas_call(functools.partial(fused_kernel, (n, local_count, capacity,...  141 us

profile of v4, /device:TPU:8, one launch (start us, length us, event | category | flops | bytes accessed | tf_op | source)
XLA Modules:
  0.0 142.4 jit_solution(10280829713338985449)
XLA Ops:
  0.0 141.4 %shard_map.100 = bf16[256,2048]{1,0:T(8,128)(2,1)S(1)} custom-call(bf16[256,2048]{1,0:T(8,128)(2,1)} %stream_hbm.1, f32[1,2048]{1,0:T(1,128)} %bitcast.3, s32[4,256]{1,0:T(4,128)} %bitcast.4, f32[4,256]{1,0:T(4,128)} %bitcast.5, bf16[2,2048,512]{2,1,0:T(8,128)(2,1)} %wg_hbm.1, bf16[2,2048,512]{2,1,0:T(8,128)(2,1)} %wu_hbm.1, bf16[2,512,2048]{2,1,0:T(8,128)(2,1)} %wd_hbm.1, ...), custom_call_target="tpu_custom_call" | custom-call | tf_op jit(solution)/shard_map/pallas_call | solution.py:514
  141.4 1.0 copy.12

commit v5 on v4

--- a/solution.py
+++ b/solution.py
@@ -98,7 +98,7 @@
     3070, 4221, 4135, 4277, 4170, 4171, 2060, 4172, 4275, 4276, 1143, 3060, 2010, 4274, 1147, 4260,
     1146, 4262, 4261, 3010, 4173, 1155, 1154, 4264, 4266, 2050, 4113, 4265, 4263, 4114, 4267, 3050,
     2040, 4252, 4110, 4251, 4153, 4157, 3040, 4250, 4145, 4156, 4241, 4144, 4243, 4242, 4255, 4111,
-    4116, 4254, 4246, 4115, 4247, 4117, 4130, 4112, 4240, 5004, 4225, 5003, 5001, 5000, 5006, 4220,
+    4116, 4254, 4246, 4115, 4247, 4117, 4130, 4112, 4240, 5004, 4225, 5000, 5003, 5001, 5006, 4220,
     5007, 5005, 5002,
 )
 MIDDLE = (
@@ -106,7 +106,7 @@
     1404, 1027, 1407, 1022, 1024, 1303, 2020, 1406, 1340, 1361, 1037, 1034, 1325, 1402, 1322, 1061,
     1400, 1367, 1364, 1063, 1422, 1415, 1405, 1300, 1362, 1062, 1366, 1421, 3020, 1307, 1423, 1363,
     1060, 1435, 2000, 1074, 1077, 1426, 2030, 1410, 2060, 1075, 1076, 1065, 1431, 1067, 1347, 1064,
-    1434, 1066, 1433, 1301, 1043, 1304, 1342, 3030, 3060, 1046, 2070, 1047, 2040, 3000, 4337, 3040,
+    1434, 1433, 1066, 1301, 1043, 1304, 1342, 3030, 3060, 1046, 2070, 1047, 2040, 3000, 4337, 3040,
     1346, 3070, 1050, 1054, 4373, 1055, 4371, 4372, 1052, 4470, 4445, 4444, 2050, 4336, 1051, 1041,
     4377, 2010, 4475, 1040, 3050, 1042, 4460, 3010, 4030, 4374, 4453, 4462, 4314, 4376, 4464, 4461,
     4015, 4317, 4313, 4466, 4310, 4311, 4004, 4463, 4332, 4002, 4467, 4012, 4451, 4352, 4357, 4016,
@@ -211,8 +211,6 @@
             ]
         )
     ]
-    for load in loads[:6]:
-        load.start()
 
     def remote(src, dst, send, recv, peer):
         return pltpu.make_async_remote_copy(
@@ -387,6 +385,9 @@
     @when_role("C")
     def _():
         begin("C", 4)
+
+    for load in loads[:6]:
+        load.start()
 
     def hidden_of(x, slot):
         gate = jnp.dot(x, wg[slot], preferred_element_type=jnp.float32)
@@ -485,19 +486,25 @@
 
     lax.fori_loop(0, 8, block, 0)
 
-    for role in PLANS:
-        @when_role(role)
-        def _():
-            run_segment(role, 9)
-            for copy in walks[role].copies:
-                copy().wait_send()
-
     def drain(g, carry):
         for copy in sibling_copies(g) + (pair_copy(g),):
             copy.wait_send()
         return carry
 
-    lax.fori_loop(0, 8, drain, 0)
+    for role in PLANS:
+        @when_role(role)
+        def _():
+            walk, steps = walks[role], segments[role][9]
+            for step in steps[:-4]:
+                walk.run(step)
+            old = len(walk.copies) - 24
+            for copy in walk.copies[:old]:
+                copy().wait_send()
+            lax.fori_loop(0, 8, drain, 0)
+            for step in steps[-4:]:
+                walk.run(step)
+            for copy in walk.copies[old:]:
+                copy().wait_send()
 
 
 def fused_device(

time: 143 us -> 142 us (level)
  no operation moved by 1% of the time
where the time goes in v5:
time: 142 us
  Pallas kernels  141 us (99%)
    pallas_call x1, Pallas kernels, fused_device(): pl.pallas_call(functools.partial(fused_kernel, (n, local_count, capacity,...  141 us

profile of v5, /device:TPU:8, one launch (start us, length us, event | category | flops | bytes accessed | tf_op | source)
XLA Modules:
  0.0 142.1 jit_solution(8748924980442814355)
XLA Ops:
  0.0 141.2 %shard_map.100 = bf16[256,2048]{1,0:T(8,128)(2,1)S(1)} custom-call(bf16[256,2048]{1,0:T(8,128)(2,1)} %stream_hbm.1, f32[1,2048]{1,0:T(1,128)} %bitcast.3, s32[4,256]{1,0:T(4,128)} %bitcast.4, f32[4,256]{1,0:T(4,128)} %bitcast.5, bf16[2,2048,512]{2,1,0:T(8,128)(2,1)} %wg_hbm.1, bf16[2,2048,512]{2,1,0:T(8,128)(2,1)} %wu_hbm.1, bf16[2,512,2048]{2,1,0:T(8,128)(2,1)} %wd_hbm.1, ...), custom_call_target="tpu_custom_call" | custom-call | tf_op jit(solution)/shard_map/pallas_call | solution.py:521
  141.2 1.0 copy.12
